TPU v7x, 32 devices: a whole 2x2x4 slice. The times are simulated.
32 devices in a mesh: sp: 8 (over z, y), tp: 4 (over x, core).
Axes of the slice: x: 2, y: 2, z: 4, core: 2. Of those that a mesh axis runs over, the one named last changes fastest.
Arguments:
- tokens: bfloat16 [2, 4096, 2048], P(None, ('sp', 'tp')), may hold values from -6.5 to 6.5, as said below
- norm_gain: float32 [2048], replicated, may hold values from 0.1 to 1.9
- w_gate: bfloat16 [2048, 4096], P('sp', 'tp'), may hold values from -0.125 to 0.125
- w_value: bfloat16 [2048, 4096], P('sp', 'tp'), may hold values from -0.125 to 0.125
- w_write: bfloat16 [2048, 512], P('sp', 'tp'), may hold values from -0.125 to 0.125
- w_read: bfloat16 [2048, 512], P('sp', 'tp'), may hold values from -0.125 to 0.125
- w_step: bfloat16 [2048, 64], replicated, may hold values from -0.125 to 0.125
- conv_value: float32 [4, 4096], replicated, may hold values from -3 to 3
- conv_write: float32 [4, 512], replicated, may hold values from -3 to 3
- conv_read: float32 [4, 512], replicated, may hold values from -3 to 3
- step_bias: float32 [64], replicated, as said below
- decay_log: float32 [64], replicated, may hold values from 0 to 0.7
- skip_gain: float32 [64], replicated, may hold values from 0.1 to 1.9
- out_gain: float32 [4096], replicated, may hold values from 0.1 to 1.9
- w_out: bfloat16 [4096, 2048], P(None, 'sp'), may hold values from -0.09375 to 0.09375
Outputs:
- mixed: bfloat16 [2, 4096, 2048], P(None, ('sp', 'tp'))
Inputs may be any that keep to these rules, and one draw needn't show every extreme that they name: `tokens`: activations of order one whose mean along a direction drifts slowly over each sequence. `step_bias`: even heads take step offsets between -5.8 and -5.0, odd heads offsets near log(0.12 to 0.33) - log(4096).
All inputs are finite; a program needn't handle non-finite values.
Results may differ from a plain program's by a relative error of at most 0.005.
The roundings to bfloat16 on the way count: a program that leaves them out, or rounds other values in their place, can miss the bound.
Values may be sent and summed in bfloat16 or wider, within the bound.
A program may use at most 192 MiB of HBM per device.

v0:
```python
import jax
import jax.numpy as jnp
from jax import lax
from jax.sharding import PartitionSpec as P

BLOCK = 64
EPSILON = 1e-06
HIGHEST = lax.Precision.HIGHEST


def shifted(x, axis, by):
    devices = lax.axis_size(axis)
    pairs = [(i, i + by) for i in range(devices) if 0 <= i + by < devices]
    return lax.ppermute(x, axis, pairs)


def entering(part, axis, combine, identity):
    place = lax.axis_index(axis)
    gathered = jax.tree.map(lambda a: lax.all_gather(a, axis), part)
    state = jax.tree.map(lambda a, e: jnp.zeros_like(a) + jnp.asarray(e, a.dtype), part, identity)

    def one(step, state):
        return combine(
            state, jax.tree.map(lambda a: lax.dynamic_index_in_dim(a, step, 0, False), gathered)
        )

    return lax.fori_loop(0, place, one, state)


def rms_scale(values, gain_vec):
    return (
        values * lax.rsqrt(jnp.mean(values * values, axis=-1, keepdims=True) + EPSILON) * gain_vec
    )


def convolve(local_rows, earlier, kernel):
    tap_count = kernel.shape[0]
    length = local_rows.shape[1]
    padded = jnp.concatenate([earlier, local_rows], axis=1).astype(jnp.float32)
    running = padded[:, 0:length, :] * kernel[0]
    for offset in range(1, tap_count):
        running = running + padded[:, offset : offset + length, :] * kernel[offset]
    return jax.nn.silu(running)


def merge_states(earlier, later):
    return (earlier[0] * later[0], earlier[1] * later[0][:, :, None, None] + later[1])


def body(
    tokens,
    norm_gain,
    w_gate,
    w_value,
    w_write,
    w_read,
    w_step,
    conv_value,
    conv_write,
    conv_read,
    step_bias,
    decay_log,
    skip_gain,
    out_gain,
    w_out,
):
    seq_count, own_rows, model_width = tokens.shape
    group_devs = lax.axis_size("tp")
    tp_rank = lax.axis_index("tp")
    head_count = w_step.shape[1]
    local_heads = head_count // group_devs
    channels = w_gate.shape[1]
    head_dim = channels // local_heads
    state_dim = w_write.shape[1]
    tap_count = conv_value.shape[0]
    group_rows = own_rows * group_devs
    normed = rms_scale(tokens.astype(jnp.float32), norm_gain).astype(jnp.bfloat16)
    whole_gate, whole_value, whole_write, whole_read, whole_out = (
        lax.all_gather(w_gate, "sp", axis=0, tiled=True),
        lax.all_gather(w_value, "sp", axis=0, tiled=True),
        lax.all_gather(w_write, "sp", axis=0, tiled=True),
        lax.all_gather(w_read, "sp", axis=0, tiled=True),
        lax.all_gather(w_out, "sp", axis=1, tiled=True),
    )
    first_head = tp_rank * local_heads
    step_cols = lax.dynamic_slice_in_dim(w_step, first_head, local_heads, 1)
    projections = (whole_gate, whole_value, whole_write, whole_read)

    def empty_rows(cols, dtype):
        return jnp.zeros((seq_count, group_rows, cols), dtype)

    initial = (
        empty_rows(channels, jnp.bfloat16),
        empty_rows(channels, jnp.bfloat16),
        empty_rows(state_dim, jnp.bfloat16),
        empty_rows(state_dim, jnp.bfloat16),
        empty_rows(local_heads, jnp.float32),
    )
    shard_piece = lax.all_gather(normed, "tp", axis=1, tiled=True)
    piece_rows = shard_piece.shape[1]
    flat_piece = shard_piece.reshape(seq_count * piece_rows, model_width)
    updated = []
    for target, weight in zip(initial[:4], projections):
        projected = jnp.dot(flat_piece, weight, preferred_element_type=jnp.float32)
        projected = projected.astype(jnp.bfloat16).reshape(seq_count, piece_rows, weight.shape[1])
        updated.append(projected)
    step_piece = jnp.dot(flat_piece, step_cols, preferred_element_type=jnp.float32)
    step_piece = step_piece.reshape(seq_count, piece_rows, local_heads)
    updated.append(step_piece)
    gate_in, value_in, write_in, read_in, step_raw = tuple(updated)
    keep_from = group_rows - tap_count + 1
    tail_rows = jnp.concatenate(
        [value_in[:, keep_from:], write_in[:, keep_from:], read_in[:, keep_from:]], axis=2
    )
    before = shifted(tail_rows, "sp", 1)
    kernel_value = lax.dynamic_slice_in_dim(conv_value, first_head * head_dim, channels, 1)
    kernel_write = lax.dynamic_slice_in_dim(conv_write, tp_rank * state_dim, state_dim, 1)
    kernel_read = lax.dynamic_slice_in_dim(conv_read, tp_rank * state_dim, state_dim, 1)
    value_conv = convolve(value_in, before[:, :, :channels], kernel_value)
    write_conv = convolve(write_in, before[:, :, channels : channels + state_dim], kernel_write)
    read_conv = convolve(read_in, before[:, :, channels + state_dim :], kernel_read)
    step_size = jax.nn.softplus(
        step_raw + lax.dynamic_slice_in_dim(step_bias, first_head, local_heads, 0)
    )
    decay_rate = -jnp.exp(lax.dynamic_slice_in_dim(decay_log, first_head, local_heads, 0))
    skip_local = lax.dynamic_slice_in_dim(skip_gain, first_head, local_heads, 0)
    block_count = group_rows // BLOCK
    value_blocks = value_conv.reshape(seq_count, block_count, BLOCK, local_heads, head_dim)
    step_blocks = jnp.moveaxis(step_size.reshape(seq_count, block_count, BLOCK, local_heads), 3, 2)
    write_blocks = write_conv.reshape(seq_count, block_count, BLOCK, state_dim)
    read_blocks = read_conv.reshape(seq_count, block_count, BLOCK, state_dim)
    log_decay = jnp.cumsum(step_blocks * decay_rate[:, None], axis=3)
    value_steps = value_blocks * jnp.moveaxis(step_blocks, 3, 2)[..., None]
    causal_mask = jnp.arange(BLOCK)[:, None] >= jnp.arange(BLOCK)[None, :]
    log_gap = log_decay[..., :, None] - log_decay[..., None, :]
    weights = jnp.exp(jnp.where(causal_mask, log_gap, -jnp.inf))
    intersect = jnp.einsum("skln,skmn->sklm", read_blocks, write_blocks, precision=HIGHEST)
    scores = weights * intersect[:, :, None]
    inner = jnp.einsum("skhlm,skmhp->sklhp", scores, value_steps, precision=HIGHEST)
    block_decay = log_decay[..., -1]
    fade_out = jnp.exp(block_decay[..., None] - log_decay)
    states = jnp.einsum(
        "skmn,skhm,skmhp->skhpn", write_blocks, fade_out, value_steps, precision=HIGHEST
    )
    run_sum = jnp.cumsum(block_decay, axis=1)
    run_before = run_sum - block_decay
    block_ids = jnp.arange(block_count)
    later_mask = (block_ids[:, None] > block_ids[None, :])[:, :, None]
    between = jnp.exp(
        jnp.where(later_mask, run_before[:, :, None, :] - run_sum[:, None, :, :], -jnp.inf)
    )
    prev_state = jnp.einsum("skjh,sjhpn->skhpn", between, states, precision=HIGHEST)
    total_fade = jnp.exp(run_sum[:, -1:, :] - run_sum)
    dev_state = jnp.einsum("sjh,sjhpn->shpn", total_fade, states, precision=HIGHEST)
    dev_decay = jnp.exp(run_sum[:, -1, :])
    identity = (jnp.ones_like(dev_decay), jnp.zeros_like(dev_state))
    incoming = entering((dev_decay, dev_state), "sp", merge_states, identity)[1]
    read_scale = jnp.exp(log_decay)
    local_part = jnp.einsum(
        "skln,skhpn,skhl->sklhp", read_blocks, prev_state, read_scale, precision=HIGHEST
    )
    outer_part = jnp.einsum(
        "skln,shpn,skhl->sklhp",
        read_blocks,
        incoming,
        jnp.exp(run_before[..., None] + log_decay),
        precision=HIGHEST,
    )
    carried = local_part + outer_part
    heads_out = (inner + carried + skip_local[:, None] * value_blocks).reshape(
        seq_count, group_rows, channels
    )
    gated = (heads_out * jax.nn.silu(gate_in.astype(jnp.float32))).astype(jnp.bfloat16)
    token_rows = lax.all_to_all(gated, "tp", split_axis=1, concat_axis=2, tiled=True)
    mixed_in = rms_scale(token_rows.astype(jnp.float32), out_gain).astype(jnp.bfloat16)
    flat_mixed = mixed_in.reshape(seq_count * own_rows, mixed_in.shape[2])
    result = jnp.dot(flat_mixed, whole_out, preferred_element_type=jnp.float32).astype(jnp.bfloat16)
    return result.reshape(seq_count, own_rows, model_width)


def solution(mesh):
    in_specs = (
        P(None, ("sp", "tp"), None),
        P(),
        P("sp", "tp"),
        P("sp", "tp"),
        P("sp", "tp"),
        P("sp", "tp"),
        P(),
        P(),
        P(),
        P(),
        P(),
        P(),
        P(),
        P(),
        P(None, "sp"),
    )
    out_specs = P(None, ("sp", "tp"), None)
    return jax.shard_map(body, mesh=mesh, in_specs=in_specs, out_specs=out_specs, check_vma=False)
```

profile of v0, /device:TPU:0, one launch (start us, length us, event | category | flops | bytes accessed | tf_op | source)
XLA Modules:
  0.0 570.5 jit_solution(64083504945850999)
XLA Ops:
  6.6 1.6 fusion.33
  8.2 2.5 fusion.35
  10.8 0.7 all-gather.10.cloned.1.call-update
  11.5 0.7 all-gather.12.cloned.1.call-update
  12.4 33.1 %all_gather.30 = bf16[2048,128]{1,0:T(8,128)(2,1)S(1)} all-gather(bf16[256,128]{1,0:T(8,128)(2,1)S(1)} %copy-done.10), channel_id=1, replica_groups=mesh['sp'=8,'tp'=4] {'sp'}, dimensions={0}, use_global_device_ids=true | all-gather | bytes 589824 | tf_op jit(solution)/shard_map/all_gather | solution.py:81
  45.5 32.9 %all_gather.31 = bf16[2048,128]{1,0:T(8,128)(2,1)S(1)} all-gather(bf16[256,128]{1,0:T(8,128)(2,1)S(1)} %copy-done.11), channel_id=1, replica_groups=mesh['sp'=8,'tp'=4] {'sp'}, dimensions={0}, use_global_device_ids=true | all-gather | bytes 589824 | tf_op jit(solution)/shard_map/all_gather | solution.py:82
  78.4 1.3 constant_dynamic-slice_fusion.1
  79.7 0.6 slice_bitcast_fusion.3
  80.3 1.6 constant_dynamic-slice_fusion
  81.9 3.4 compare_select_fusion
  85.4 3.5 reduce_window_sum.24
  89.4 3.6 convolution_convert_fusion.4
  93.0 1.2 convolution_convert_fusion.3
  95.1 0.8 exponential_bitcast_fusion.2
  96.0 28.8 %all-gather.10.cloned.1.call-done = bf16[2048,1024]{1,0:T(8,128)(2,1)} async-done(((bf16[256,1024]{1,0:T(8,128)(2,1)}), bf16[2048,1024]{1,0:T(8,128)(2,1)}) %all-gather.10.cloned.1.call-update) | async-done | bytes 4194320 | tf_op jit(solution)/shard_map/all_gather | solution.py:80
  124.8 7.9 %convolution_convert_fusion.2 = bf16[1024,1024]{1,0:T(8,128)(2,1)S(1)} fusion(bf16[1024,2048]{1,0:T(8,128)(2,1)} %bitcast.120, bf16[2048,1024]{1,0:T(8,128)(2,1)} %all-gather.10.cloned.1.call-done), kind=kOutput, calls=%fused_computation.53 | convolution fusion | flops 4296015872 | bytes 10485760 | tf_op jit(solution)/shard_map/dot_general | solution.py:104
  132.7 0.6 pad_maximum_fusion
  133.4 3.1 collective-permute-start
  136.4 0.6 fusion.63
  137.2 1.1 copy.101
  138.3 0.8 copy.119
  139.1 0.7 slice.132
  139.9 0.6 maximum_convert_fusion
  140.5 4.6 divide_multiply_fusion
  145.1 7.4 %reshape.114 = f32[2,8,64,16,64]{4,3,2,1,0:T(8,128)} reshape(f32[2,512,1024]{2,1,0:T(8,128)} %divide_multiply_fusion) | data formatting | bytes 8388608 | tf_op jit(solution)/shard_map/reshape | solution.py:128
  152.5 0.7 fusion.62
  153.7 9.0 %broadcast_multiply_fusion = (f32[2,8,64,16,64]{4,3,2,1,0:T(8,128)S(1)}, f32[2,8,64,16,64]{4,3,2,1,0:T(8,128)}) fusion(f32[2,8,64,16]{3,2,1,0:T(8,128)S(1)} %copy.101, f32[2,8,64,16,64]{4,3,2,1,0:T(8,128)} %reshape.114, f32[2,8,64,16]{3,2,1,0:T(8,128)S(1)} %copy.98), kind=kLoop, calls=%fused_computation.33 | loop fusion | flops 2097152 | bytes 12713984 | tf_op jit(solution)/shard_map/skmn,skhm,skmhp->skhpn/dot_general | solution.py:142
  162.7 15.2 %fusion.3 = f32[2,8,16,64,128]{4,3,2,1,0:T(8,128)S(1)} fusion(f32[2,8,64,128,1]{3,2,4,1,0:T(8,128)S(1)} %bitcast.117, f32[2,8,64,16,64]{4,3,2,1,0:T(8,128)S(1)} %get-tuple-element.60), kind=kOutput, calls=%fused_computation.6 | convolution fusion | flops 1610612736 | bytes 13107200 | tf_op jit(solution)/shard_map/skmn,skhm,skmhp->skhpn/dot_general | solution.py:142
  177.9 11.7 %fusion.11 = f32[2,16,1,64,128]{4,2,3,1,0:T(1,128)} fusion(f32[2,8,16,1,1]{1,3,4,2,0:T(1,128)S(1)} %copy.119, f32[2,8,16,64,128]{4,3,2,1,0:T(8,128)S(1)} %fusion.3), kind=kOutput, calls=%fused_computation.14 | convolution fusion | flops 25165824 | bytes 9438208 | tf_op jit(solution)/shard_map/sjh,sjhpn->shpn/dot_general | solution.py:154
  190.5 18.6 %all-gather = f32[16,1,16]{2,1,0:T(1,128)S(1)} all-gather(f32[2,1,16]{2,1,0:T(1,128)S(1)} %copy-done.13), channel_id=2, replica_groups=mesh['sp'=8,'tp'=4] {'sp'}, dimensions={0}, use_global_device_ids=true | all-gather | bytes 1152 | tf_op jit(solution)/shard_map/all_gather | solution.py:19
  209.1 9.4 %convolution_convert_fusion.1 = bf16[1024,1024]{1,0:T(8,128)(2,1)} fusion(bf16[1024,2048]{1,0:T(8,128)(2,1)} %bitcast.121, bf16[2048,1024]{1,0:T(8,128)(2,1)} %all-gather.12.cloned.1.call-done), kind=kOutput, calls=%fused_computation.52 | convolution fusion | flops 4296015872 | bytes 10485760 | tf_op jit(solution)/shard_map/dot_general | solution.py:104
  218.4 9.2 %copy.110 = f32[2,8,64,16,64]{2,4,3,1,0:T(8,128)} copy(f32[2,8,64,16,64]{4,3,2,1,0:T(8,128)} %reshape.114) | data formatting | bytes 8388608 | tf_op jit(solution)/shard_map/reshape | solution.py:128
  228.0 0.9 fusion.65
  228.9 17.3 %fusion.30 = f32[2,8,16,64,128]{4,1,3,2,0:T(8,128)} fusion(f32[2,8,16,64,128]{4,3,2,1,0:T(8,128)} %copy-done.2, f32[2,8,16]{1,2,0:T(8,128)S(1)} %copy.104, f32[2,8,16]{1,2,0:T(8,128)S(1)} %copy.103, pred[8,8]{1,0:T(8,128)(4,1)S(1)} %iota_compare_fusion.1), kind=kOutput, calls=%fused_computation.42 | convolution fusion | flops 201330688 | bytes 16779328 | tf_op jit(solution)/shard_map/skjh,sjhpn->skhpn/dot_general | solution.py:152
  246.2 17.5 %fusion.5 = f32[2,8,16,64,64]{4,3,2,1,0:T(8,128)} fusion(f32[2,8,64,16,64]{4,3,2,1,0:T(8,128)S(1)} %bitcast.111, f32[2,8,64,64]{3,2,1,0:T(8,128)S(1)} %fusion.65, f32[2,8,16,64]{3,2,1,0:T(8,128)S(1)} %reduce_window_sum.24, pred[64,64]{1,0:T(8,128)(4,1)S(1)} %iota_compare_fusion), kind=kOutput, calls=%fused_computation.8 | convolution fusion | flops 808452096 | bytes 8720384 | tf_op jit(solution)/shard_map/skhlm,skmhp->sklhp/dot_general | solution.py:139
  263.8 60.0 %all-gather.16.cloned.1.call-done = f32[16,16,64,128]{3,2,1,0:T(8,128)} async-done(((f32[2,16,64,128]{3,2,1,0:T(8,128)}), f32[16,16,64,128]{3,2,1,0:T(8,128)}) %all-gather.16.cloned.1.call-update) | async-done | bytes 8388624 | tf_op jit(solution)/shard_map/all_gather | solution.py:19
  323.9 9.5 %fusion.38 = f32[2,8,64,16,64]{2,4,3,1,0:T(8,128)} fusion(f32[2,8,64,128,1]{3,2,4,1,0:T(8,128)S(1)} %bitcast.115, f32[2,16,64,128]{3,2,1,0:T(8,128)S(1)} %get-tuple-element.49), kind=kOutput, calls=%fused_computation.57 | convolution fusion | flops 1610612736 | bytes 5767168 | tf_op jit(solution)/shard_map/skln,shpn,skhl->sklhp/dot_general | solution.py:162
  333.4 19.5 %fusion = f32[2,8,64,16,64]{2,4,3,1,0:T(8,128)} fusion(f32[2,8,16,64,64]{4,3,2,1,0:T(8,128)} %fusion.5, f32[2,8,64,16,64]{2,4,3,1,0:T(8,128)} %copy.110, f32[2,8,64,16,64]{2,4,3,1,0:T(8,128)} %fusion.38, f32[16]{0:T(128)S(1)} %dynamic_slice.37, f32[2,8,64,16]{2,3,1,0:T(8,128)S(1)} %copy-done.5, f32[2,8,64,16]{2,3,1,0:T(8,128)S(1)} %get-tuple-element.62, ...), kind=kOutput, calls=%fused_computation.3 | convolution fusion | flops 1616904192 | bytes 25821248 | tf_op jit(solution)/shard_map/skln,skhpn,skhl->sklhp/dot_general | solution.py:159
  352.9 9.2 %copy.111 = f32[2,8,64,16,64]{4,3,2,1,0:T(8,128)} copy(f32[2,8,64,16,64]{2,4,3,1,0:T(8,128)} %fusion) | data formatting | bytes 8388608 | tf_op jit(solution)/shard_map/add | solution.py:170
  362.1 8.0 %reshape.117 = f32[2,512,1024]{2,1,0:T(8,128)} reshape(f32[2,8,64,16,64]{4,3,2,1,0:T(8,128)} %copy.111) | data formatting | bytes 8388608 | tf_op jit(solution)/shard_map/reshape | solution.py:170
  370.1 3.5 fusion.26
  373.6 2.2 copy.112
  375.8 28.3 %all_to_all.4 = bf16[2,512,1024]{2,0,1:T(2,128)(2,1)S(1)} all-to-all(bf16[2,512,1024]{2,0,1:T(2,128)(2,1)S(1)} %copy.112), channel_id=1, replica_groups=mesh['sp'=8,'tp'=4] {'tp'}, dimensions={1} | all-to-all | bytes 4194304 | tf_op jit(solution)/shard_map/all_to_all | solution.py:174
  404.1 1.6 copy.113
  405.7 5.8 %copy.123 = f32[32,8,4,1024]{3,1,2,0:T(8,128)} copy(f32[32,8,4,1024]{3,2,1,0:T(4,128)S(1)} %bitcast.113) | data formatting | bytes 8388608
  411.5 2.2 multiply_reduce_fusion
  413.9 137.3 %all-gather.14.cloned.1.call-done = bf16[4096,2048]{1,0:T(8,128)(2,1)} async-done(((bf16[4096,256]{1,0:T(8,128)(2,1)}), bf16[4096,2048]{1,0:T(8,128)(2,1)}) %all-gather.14.cloned.1.call-update) | async-done | bytes 16777232 | tf_op jit(solution)/shard_map/all_gather | solution.py:83
  551.2 12.6 %convolution_convert_fusion = bf16[256,2048]{1,0:T(8,128)(2,1)} fusion(bf16[4096,2048]{1,0:T(8,128)(2,1)} %all-gather.14.cloned.1.call-done, f32[256,4096]{1,0:T(8,128)} %bitcast.124, f32[4096]{0:T(1024)S(1)} %copy-done.18, f32[256]{0:T(256)S(1)} %bitcast.141), kind=kOutput, calls=%fused_computation.45 | convolution fusion | flops 4298637312 | bytes 22037504 | tf_op jit(solution)/shard_map/dot_general | solution.py:177
  (88 shorter events, 3.8 us)
Async XLA Ops:
  6.5 75.3 %copy-start = (bf16[2048,64]{0,1:T(8,128)(2,1)S(1)}, bf16[2048,64]{0,1:T(8,128)(2,1)}, u32[]{:S(2)}) copy-start(bf16[2048,64]{0,1:T(8,128)(2,1)} %param.23) | copy-start | bytes 786436
  6.5 5.7 %copy-start.19 = (f32[64]{0:T(128)S(1)}, f32[64]{0:T(128)}, u32[]{:S(2)}) copy-start(f32[64]{0:T(128)} %param.27) | copy-start | bytes 772
  6.5 5.8 %copy-start.20 = (f32[64]{0:T(128)S(1)}, f32[64]{0:T(128)}, u32[]{:S(2)}) copy-start(f32[64]{0:T(128)} %param.28) | copy-start | bytes 772
  6.5 5.9 %copy-start.10 = (bf16[256,128]{1,0:T(8,128)(2,1)S(1)}, bf16[256,128]{1,0:T(8,128)(2,1)}, u32[]{:S(2)}) copy-start(bf16[256,128]{1,0:T(8,128)(2,1)} %param.21) | copy-start | bytes 196612
  6.5 39.0 %copy-start.11 = (bf16[256,128]{1,0:T(8,128)(2,1)S(1)}, bf16[256,128]{1,0:T(8,128)(2,1)}, u32[]{:S(2)}) copy-start(bf16[256,128]{1,0:T(8,128)(2,1)} %param.22) | copy-start | bytes 196612
  6.5 75.3 %all-gather.8.cloned.1.call-start = ((), (), s32[]{:S(2)}) async-start(), calls=%async_computation.1 | async-start | bytes 5242880 | tf_op jit(solution)/shard_map/all_gather | solution.py:99
  10.7 114.0 %all-gather.10.cloned.1.call-start = ((), (), s32[]{:S(2)}) async-start(), calls=%async_computation.2 | async-start | bytes 4718592 | tf_op jit(solution)/shard_map/all_gather | solution.py:80
  11.5 197.6 %all-gather.12.cloned.1.call-start = ((), (), s32[]{:S(2)}) async-start(), calls=%async_computation.3 | async-start | bytes 4718592 | tf_op jit(solution)/shard_map/all_gather | solution.py:79
  12.2 311.5 %all-gather.16.cloned.1.call-start = ((), (), s32[]{:S(2)}) async-start(), calls=%async_computation.5 | async-start | bytes 9437184 | tf_op jit(solution)/shard_map/all_gather | solution.py:19
  89.4 3.6 copy-start.3
  93.0 1.5 copy-start.6
  94.3 1.7 copy-start.8
  133.4 5.8 %collective-permute-start = (bf16[2,3,1280]{2,1,0:T(4,128)(2,1)}, bf16[2,3,1280]{2,1,0:T(4,128)(2,1)}, u32[]{:S(2)}, u32[]{:S(2)}) collective-permute-start(bf16[2,3,1280]{2,1,0:T(4,128)(2,1)} %pad_maximum_fusion), channel_id=1, source_target_pairs={{0,4},{4,8},{8,12},{12,16},{16,20},{20,24},{24,28},{1,5},{5,9},{9,... | collective-permute-start | bytes 46088 | tf_op jit(solution)/shard_map/ppermute | solution.py:14
  145.1 8.1 %copy-start.7 = (bf16[1024,128]{1,0:T(8,128)(2,1)S(1)}, bf16[1024,128]{1,0:T(8,128)(2,1)}, u32[]{:S(2)}) copy-start(bf16[1024,128]{1,0:T(8,128)(2,1)} %copy-done.6) | copy-start | bytes 786436
  145.1 8.1 %copy-start.9 = (bf16[1024,128]{1,0:T(8,128)(2,1)S(1)}, bf16[1024,128]{1,0:T(8,128)(2,1)}, u32[]{:S(2)}) copy-start(bf16[1024,128]{1,0:T(8,128)(2,1)} %copy-done.8) | copy-start | bytes 786436
  145.1 8.2 %copy-start.14 = (f32[128]{0:T(128)S(1)}, f32[128]{0:T(128)}, u32[]{:S(2)}) copy-start(f32[128]{0:T(128)} %get-tuple-element.75) | copy-start | bytes 1540
  145.1 8.2 %copy-start.15 = (f32[128]{0:T(128)S(1)}, f32[128]{0:T(128)}, u32[]{:S(2)}) copy-start(f32[128]{0:T(128)} %get-tuple-element.76) | copy-start | bytes 1540
  145.1 8.2 %copy-start.16 = (f32[128]{0:T(128)S(1)}, f32[128]{0:T(128)}, u32[]{:S(2)}) copy-start(f32[128]{0:T(128)} %get-tuple-element.77) | copy-start | bytes 1540
  145.1 8.2 %copy-start.17 = (f32[128]{0:T(128)S(1)}, f32[128]{0:T(128)}, u32[]{:S(2)}) copy-start(f32[128]{0:T(128)} %get-tuple-element.78) | copy-start | bytes 1540
  177.8 11.7 %copy-start.2 = (f32[2,8,16,64,128]{4,3,2,1,0:T(8,128)}, f32[2,8,16,64,128]{4,3,2,1,0:T(8,128)S(1)}, u32[]{:S(2)}) copy-start(f32[2,8,16,64,128]{4,3,2,1,0:T(8,128)S(1)} %fusion.3) | copy-start | bytes 25165828
  177.9 12.3 %copy-start.21 = (f32[64]{0:T(128)S(1)}, f32[64]{0:T(128)}, u32[]{:S(2)}) copy-start(f32[64]{0:T(128)} %param.29) | copy-start | bytes 772
  177.9 12.4 %copy-start.12 = (f32[4,128]{1,0:T(4,128)S(1)}, f32[4,128]{1,0:T(4,128)}, u32[]{:S(2)}) copy-start(f32[4,128]{1,0:T(4,128)} %get-tuple-element.86) | copy-start | bytes 6148
  177.9 12.6 %copy-start.13 = (f32[2,1,16]{2,1,0:T(1,128)S(1)}, f32[2,1,16]{2,1,0:T(1,128)}, u32[]{:S(2)}) copy-start(f32[2,1,16]{2,1,0:T(1,128)} %get-tuple-element.74) | copy-start | bytes 388
  189.6 361.6 %all-gather.14.cloned.1.call-start = ((), (), s32[]{:S(2)}) async-start(), calls=%async_computation.4 | async-start | bytes 18874368 | tf_op jit(solution)/shard_map/all_gather | solution.py:83
  227.9 18.3 %slice-start = ((s8[8388608]{0:T(1024)(128)(4,1)}), s8[4194304]{0:T(1024)(128)(4,1)S(1)}, s32[]{:S(2)}) async-start(s8[8388608]{0:T(1024)(128)(4,1)} %bitcast.110), calls=%async_computation.6 | async-start | bytes 8388608
  228.9 17.3 %slice-start.1 = ((s8[8388608]{0:T(1024)(128)(4,1)}), s8[4194304]{0:T(1024)(128)(4,1)S(1)}, s32[]{:S(2)}) async-start(s8[8388608]{0:T(1024)(128)(4,1)} %bitcast.110), calls=%async_computation.7 | async-start | bytes 8388608
  323.9 9.5 %copy-start.5 = (f32[2,8,64,16]{2,3,1,0:T(8,128)S(1)}, f32[2,8,64,16]{2,3,1,0:T(8,128)}, u32[]{:S(2)}) copy-start(f32[2,8,64,16]{2,3,1,0:T(8,128)} %get-tuple-element.64) | copy-start | bytes 196612
  362.1 8.0 %copy-start.4 = (bf16[1024,1024]{1,0:T(8,128)(2,1)S(1)}, bf16[1024,1024]{1,0:T(8,128)(2,1)}, u32[]{:S(2)}) copy-start(bf16[1024,1024]{1,0:T(8,128)(2,1)} %convolution_convert_fusion.1) | copy-start | bytes 6291460
  405.7 145.4 %copy-start.18 = (f32[4096]{0:T(1024)S(1)}, f32[4096]{0:T(1024)}, u32[]{:S(2)}) copy-start(f32[4096]{0:T(1024)} %param.30) | copy-start | bytes 49156
  551.2 12.6 %copy-start.1 = (bf16[2048,64]{0,1:T(8,128)(2,1)S(1)}, bf16[2048,64]{0,1:T(8,128)(2,1)}, u32[]{:S(2)}) copy-start(bf16[2048,64]{0,1:T(8,128)(2,1)} %param.23) | copy-start | bytes 786436
Sparse Core Ops, SparseCore 0:
  10.8 37.1 all-gather.7
  50.2 74.5 all-gather.9
  126.9 71.7 all-gather.11
  200.7 123.0 all-gather.15
  325.6 225.4 all-gather.13
where the time goes:
time: 580 us; the launch traced here: 570 us
  waiting for transfers between devices  228 us (39%)
  matrix products  130 us (22%)
  blocking collectives  113 us (19%)
  local copies, waits for them, and re-layouts  51.9 us (9%)
  other arithmetic  30.8 us (5%)
  between operations  13.8 us (2%)
    all_gather x1, waiting for transfers between devices, body(): lax.all_gather(w_out, 'sp', axis=1, tiled=True)  137 us
    all_gather x1, waiting for transfers between devices, entering(): gathered = jax.tree.map(lambda a: lax.all_gather(a, axis), part)  60 us
    all_gather x1, blocking collectives, body(): lax.all_gather(w_write, 'sp', axis=0, tiled=True)  33.1 us
    all_gather x1, blocking collectives, body(): lax.all_gather(w_read, 'sp', axis=0, tiled=True)  32.9 us
    all_gather x1, waiting for transfers between devices, body(): lax.all_gather(w_value, 'sp', axis=0, tiled=True)  28.8 us
    all_to_all x1, blocking collectives, body(): lax.all_to_all(gated, 'tp', split_axis=1, concat_axis=2, tiled=True)  28.3 us
    dot_general x4, matrix products, body(): projected = jnp.dot(flat_piece, weight, preferred_element_type=jnp.float32)  22.1 us
    dot_general x1, matrix products, body(): jnp.einsum('skln,skhpn,skhl->sklhp', read_blocks, prev_state, read_scale,...  19.5 us
  transfers between devices with their start and end apart: 6, of which 3 were waited for; matrix products, arithmetic and copies ran while one was open for 34% of the time, Pallas kernels for 0%

commit v1 on v0

--- a/solution.py
+++ b/solution.py
@@ -6,6 +6,18 @@
 BLOCK = 64
 EPSILON = 1e-06
 HIGHEST = lax.Precision.HIGHEST
+
+
+def collect(shard, axis, dim):
+    ways, here, step = (lax.axis_size(axis), lax.axis_index(axis), shard.shape[dim])
+    shape = [n * ways if d == dim else n for d, n in enumerate(shard.shape)]
+    full = lax.dynamic_update_slice_in_dim(
+        jnp.zeros(shape, shard.dtype), shard, here * step, axis=dim
+    )
+    for far in range(1, ways):
+        shard = lax.ppermute(shard, axis, [(d, (d + 1) % ways) for d in range(ways)])
+        full = lax.dynamic_update_slice_in_dim(full, shard, (here - far) % ways * step, axis=dim)
+    return full
 
 
 def shifted(x, axis, by):
@@ -80,7 +92,7 @@
         lax.all_gather(w_value, "sp", axis=0, tiled=True),
         lax.all_gather(w_write, "sp", axis=0, tiled=True),
         lax.all_gather(w_read, "sp", axis=0, tiled=True),
-        lax.all_gather(w_out, "sp", axis=1, tiled=True),
+        collect(w_out, "sp", 1),
     )
     first_head = tp_rank * local_heads
     step_cols = lax.dynamic_slice_in_dim(w_step, first_head, local_heads, 1)

time: 580 us -> 730 us (1.26)
  the two profiles are of different devices: /device:TPU:0 before, /device:TPU:28 now
where the time goes in v1:
time: 730 us; the launch traced here: 720 us
  waiting for transfers between devices  323 us (44%)
  matrix products  129 us (18%)
  blocking collectives  105 us (14%)
  local copies, waits for them, and re-layouts  82.7 us (11%)
  other arithmetic  40.7 us (6%)
  starting transfers between devices  26 us (4%)
  between operations  13.9 us (2%)
    ppermute x7, waiting for transfers between devices, collect(): lax.ppermute(shard, axis, [(d, (d + 1) % ways) for d in range(ways)])  280 us
    all_gather x1, blocking collectives, entering(): gathered = jax.tree.map(lambda a: lax.all_gather(a, axis), part)  40.7 us
    all_gather x1, blocking collectives, body(): lax.all_gather(w_read, 'sp', axis=0, tiled=True)  33.2 us
    all_gather x1, blocking collectives, body(): lax.all_gather(w_write, 'sp', axis=0, tiled=True)  31.5 us
    all_gather x1, waiting for transfers between devices, body(): lax.all_gather(w_value, 'sp', axis=0, tiled=True)  25.8 us
    dot_general x4, matrix products, body(): projected = jnp.dot(flat_piece, weight, preferred_element_type=jnp.float32)  22.1 us
    ppermute x7, starting transfers between devices, collect(): lax.ppermute(shard, axis, [(d, (d + 1) % ways) for d in range(ways)])  21 us
    dot_general x1, matrix products, body(): jnp.einsum('skln,skhpn,skhl->sklhp', read_blocks, prev_state, read_scale,...  18.8 us
  transfers between devices with their start and end apart: 13, of which 7 were waited for; matrix products, arithmetic and copies ran while one was open for 31% of the time, Pallas kernels for 0%

profile of v1, /device:TPU:28, one launch (start us, length us, event | category | flops | bytes accessed | tf_op | source)
XLA Modules:
  0.0 720.3 jit_solution(17187487857526046789)
XLA Ops:
  6.6 1.6 fusion.33
  8.2 2.5 fusion.35
  12.4 31.5 %all_gather.27 = bf16[2048,128]{1,0:T(8,128)(2,1)S(1)} all-gather(bf16[256,128]{1,0:T(8,128)(2,1)S(1)} %copy-done.15), channel_id=1, replica_groups=mesh['sp'=8,'tp'=4] {'sp'}, dimensions={0}, use_global_device_ids=true | all-gather | bytes 589824 | tf_op jit(solution)/shard_map/all_gather | solution.py:93
  43.9 33.2 %all_gather.28 = bf16[2048,128]{1,0:T(8,128)(2,1)S(1)} all-gather(bf16[256,128]{1,0:T(8,128)(2,1)S(1)} %copy-done.16), channel_id=1, replica_groups=mesh['sp'=8,'tp'=4] {'sp'}, dimensions={0}, use_global_device_ids=true | all-gather | bytes 589824 | tf_op jit(solution)/shard_map/all_gather | solution.py:94
  80.6 3.4 compare_select_fusion
  84.2 3.5 reduce_window_sum.24
  88.2 3.6 convolution_convert_fusion.4
  94.7 25.8 %all-gather.9.cloned.1.call-done = bf16[2048,1024]{1,0:T(8,128)(2,1)} async-done(((bf16[256,1024]{1,0:T(8,128)(2,1)}), bf16[2048,1024]{1,0:T(8,128)(2,1)}) %all-gather.9.cloned.1.call-update) | async-done | bytes 4194320 | tf_op jit(solution)/shard_map/all_gather | solution.py:92
  120.6 7.9 %convolution_convert_fusion.2 = bf16[1024,1024]{1,0:T(8,128)(2,1)S(1)} fusion(bf16[1024,2048]{1,0:T(8,128)(2,1)} %bitcast.120, bf16[2048,1024]{1,0:T(8,128)(2,1)} %all-gather.9.cloned.1.call-done), kind=kOutput, calls=%fused_computation.53 | convolution fusion | flops 4296015872 | bytes 10485760 | tf_op jit(solution)/shard_map/dot_general | solution.py:116
  133.2 2.4 collective-permute-done
  136.9 4.6 divide_multiply_fusion
  141.5 7.4 %reshape.114 = f32[2,8,64,16,64]{4,3,2,1,0:T(8,128)} reshape(f32[2,512,1024]{2,1,0:T(8,128)} %divide_multiply_fusion) | data formatting | bytes 8388608 | tf_op jit(solution)/shard_map/reshape | solution.py:140
  150.1 8.7 %broadcast_multiply_fusion = (f32[2,8,64,16,64]{4,3,2,1,0:T(8,128)S(1)}, f32[2,8,64,16,64]{4,3,2,1,0:T(8,128)}) fusion(f32[2,8,64,16]{3,2,1,0:T(8,128)S(1)} %copy.101, f32[2,8,64,16,64]{4,3,2,1,0:T(8,128)} %reshape.114, f32[2,8,64,16]{3,2,1,0:T(8,128)S(1)} %copy.98), kind=kLoop, calls=%fused_computation.33 | loop fusion | flops 2097152 | bytes 12713984 | tf_op jit(solution)/shard_map/skmn,skhm,skmhp->skhpn/dot_general | solution.py:154
  158.8 15.0 %fusion.3 = f32[2,8,16,64,128]{4,3,2,1,0:T(8,128)S(1)} fusion(f32[2,8,64,128,1]{3,2,4,1,0:T(8,128)S(1)} %bitcast.117, f32[2,8,64,16,64]{4,3,2,1,0:T(8,128)S(1)} %get-tuple-element.60), kind=kOutput, calls=%fused_computation.6 | convolution fusion | flops 1610612736 | bytes 13107200 | tf_op jit(solution)/shard_map/skmn,skhm,skmhp->skhpn/dot_general | solution.py:154
  173.8 11.7 %fusion.11 = f32[2,16,1,64,128]{4,2,3,1,0:T(1,128)} fusion(f32[2,8,16,1,1]{1,3,4,2,0:T(1,128)S(1)} %copy.119, f32[2,8,16,64,128]{4,3,2,1,0:T(8,128)S(1)} %fusion.3), kind=kOutput, calls=%fused_computation.14 | convolution fusion | flops 25165824 | bytes 9438208 | tf_op jit(solution)/shard_map/sjh,sjhpn->shpn/dot_general | solution.py:166
  185.6 2.6 collective-permute-start.1
  188.2 75.4 %collective-permute-done.1 = bf16[4096,256]{1,0:T(8,128)(2,1)S(1)} collective-permute-done((bf16[4096,256]{1,0:T(8,128)(2,1)}, bf16[4096,256]{1,0:T(8,128)(2,1)S(1)}, u32[]{:S(2)}, u32[]{:S(2)}) %collective-permute-start.1) | collective-permute-done | bytes 2097184 | tf_op jit(solution)/shard_map/ppermute | solution.py:18
  264.9 5.1 collective-permute-start.2
  270.0 50.9 %collective-permute-done.2 = bf16[4096,256]{1,0:T(8,128)(2,1)S(1)} collective-permute-done((bf16[4096,256]{1,0:T(8,128)(2,1)S(1)}, bf16[4096,256]{1,0:T(8,128)(2,1)S(1)}, u32[]{:S(2)}, u32[]{:S(2)}) %collective-permute-start.2) | collective-permute-done | bytes 2097184 | tf_op jit(solution)/shard_map/ppermute | solution.py:18
  323.2 91.3 %collective-permute-done.3 = bf16[4096,256]{1,0:T(8,128)(2,1)} collective-permute-done((bf16[4096,256]{1,0:T(8,128)(2,1)S(1)}, bf16[4096,256]{1,0:T(8,128)(2,1)}, u32[]{:S(2)}, u32[]{:S(2)}) %collective-permute-start.3) | collective-permute-done | bytes 2097184 | tf_op jit(solution)/shard_map/ppermute | solution.py:18
  414.5 2.8 collective-permute-start.4
  417.4 62.3 %collective-permute-done.4 = bf16[4096,256]{1,0:T(8,128)(2,1)} collective-permute-done((bf16[4096,256]{1,0:T(8,128)(2,1)}, bf16[4096,256]{1,0:T(8,128)(2,1)}, u32[]{:S(2)}, u32[]{:S(2)}) %collective-permute-start.4) | collective-permute-done | bytes 2097184 | tf_op jit(solution)/shard_map/ppermute | solution.py:18
  479.7 5.2 collective-permute-start.5
  484.9 6.0 broadcast_in_dim.31
  496.2 3.1 constant_dynamic-update-slice_fusion.4
  499.5 40.7 %all-gather = f32[16,1,16]{2,1,0:T(1,128)S(1)} all-gather(f32[2,1,16]{2,1,0:T(1,128)S(1)} %copy-done.18), channel_id=2, replica_groups=mesh['sp'=8,'tp'=4] {'sp'}, dimensions={0}, use_global_device_ids=true | all-gather | bytes 1152 | tf_op jit(solution)/shard_map/all_gather | solution.py:31
  540.2 4.3 collective-permute-start.6
  544.5 9.3 %convolution_convert_fusion.1 = bf16[1024,1024]{1,0:T(8,128)(2,1)} fusion(bf16[1024,2048]{1,0:T(8,128)(2,1)} %bitcast.121, bf16[2048,1024]{1,0:T(8,128)(2,1)} %all-gather.11.cloned.1.call-done), kind=kOutput, calls=%fused_computation.52 | convolution fusion | flops 4296015872 | bytes 10485760 | tf_op jit(solution)/shard_map/dot_general | solution.py:116
  553.8 9.0 %copy.110 = f32[2,8,64,16,64]{2,4,3,1,0:T(8,128)} copy(f32[2,8,64,16,64]{4,3,2,1,0:T(8,128)} %reshape.114) | data formatting | bytes 8388608 | tf_op jit(solution)/shard_map/reshape | solution.py:140
  564.1 17.2 %fusion.30 = f32[2,8,16,64,128]{4,1,3,2,0:T(8,128)} fusion(f32[2,8,16,64,128]{4,3,2,1,0:T(8,128)} %copy-done.2, f32[2,8,16]{1,2,0:T(8,128)S(1)} %copy.104, f32[2,8,16]{1,2,0:T(8,128)S(1)} %copy.103, pred[8,8]{1,0:T(8,128)(4,1)S(1)} %iota_compare_fusion.1), kind=kOutput, calls=%fused_computation.42 | convolution fusion | flops 201330688 | bytes 16779328 | tf_op jit(solution)/shard_map/skjh,sjhpn->skhpn/dot_general | solution.py:164
  581.4 17.8 %fusion.5 = f32[2,8,16,64,64]{4,3,2,1,0:T(8,128)} fusion(f32[2,8,64,16,64]{4,3,2,1,0:T(8,128)S(1)} %bitcast.111, f32[2,8,64,64]{3,2,1,0:T(8,128)S(1)} %fusion.65, f32[2,8,16,64]{3,2,1,0:T(8,128)S(1)} %reduce_window_sum.24, pred[64,64]{1,0:T(8,128)(4,1)S(1)} %iota_compare_fusion), kind=kOutput, calls=%fused_computation.8 | convolution fusion | flops 808452096 | bytes 8720384 | tf_op jit(solution)/shard_map/skhlm,skmhp->sklhp/dot_general | solution.py:151
  599.3 10.5 %while.12 = (s32[]{:T(128)}, f32[2,16,64,128]{3,2,1,0:T(8,128)S(1)}, s32[]{:T(128)}, f32[8,2,16]{2,1,0:T(2,128)S(1)}, f32[8,2,16,64,128]{4,3,2,1,0:T(8,128)}, /*index=5*/s32[]{:T(128)}, s32[]{:T(128)}, s32[]{:T(128)}) while((s32[]{:T(128)}, f32[2,16,64,128]{3,2,1,0:T(8,128)S(1)}, s32[]{:T(128)}, f32[8,2,16]{2,1,0:T(2,128)S(1)}, ...), condition=%wide.region_4.5_spmd, body=%wide.region_3.4_spmd.sunk | while | flops 524293 | bytes 3146239 | solution.py:39
  609.8 9.0 %fusion.38 = f32[2,8,64,16,64]{2,4,3,1,0:T(8,128)} fusion(f32[2,8,64,128,1]{3,2,4,1,0:T(8,128)S(1)} %bitcast.115, f32[2,16,64,128]{3,2,1,0:T(8,128)S(1)} %get-tuple-element.49), kind=kOutput, calls=%fused_computation.57 | convolution fusion | flops 1610612736 | bytes 5767168 | tf_op jit(solution)/shard_map/skln,shpn,skhl->sklhp/dot_general | solution.py:174
  618.8 18.8 %fusion = f32[2,8,64,16,64]{2,4,3,1,0:T(8,128)} fusion(f32[2,8,16,64,64]{4,3,2,1,0:T(8,128)} %fusion.5, f32[2,8,64,16,64]{2,4,3,1,0:T(8,128)} %copy.110, f32[2,8,64,16,64]{2,4,3,1,0:T(8,128)} %fusion.38, f32[16]{0:T(128)S(1)} %dynamic_slice.37, f32[2,8,64,16]{2,3,1,0:T(8,128)S(1)} %copy-done.10, f32[2,8,64,16]{2,3,1,0:T(8,128)S(1)} %get-tuple-element.62, ...), kind=kOutput, calls=%fused_computation.3 | convolution fusion | flops 1616904192 | bytes 25821248 | tf_op jit(solution)/shard_map/skln,skhpn,skhl->sklhp/dot_general | solution.py:171
  637.5 9.2 %copy.111 = f32[2,8,64,16,64]{4,3,2,1,0:T(8,128)} copy(f32[2,8,64,16,64]{2,4,3,1,0:T(8,128)} %fusion) | data formatting | bytes 8388608 | tf_op jit(solution)/shard_map/add | solution.py:182
  646.7 8.0 %reshape.117 = f32[2,512,1024]{2,1,0:T(8,128)} reshape(f32[2,8,64,16,64]{4,3,2,1,0:T(8,128)} %copy.111) | data formatting | bytes 8388608 | tf_op jit(solution)/shard_map/reshape | solution.py:182
  654.7 3.5 fusion.26
  658.2 3.5 copy.112
  661.7 3.6 all-to-all-start
  665.4 3.1 constant_dynamic-update-slice_fusion.3
  668.4 3.1 constant_dynamic-update-slice_fusion.2
  671.5 3.1 constant_dynamic-update-slice_fusion.1
  674.7 3.1 constant_dynamic-update-slice_fusion
  677.8 13.2 %all-to-all-done = bf16[2,512,1024]{2,0,1:T(2,128)(2,1)S(1)} async-done(((bf16[2,512,1024]{2,0,1:T(2,128)(2,1)}), bf16[2,512,1024]{2,0,1:T(2,128)(2,1)S(1)}, u32[]{:S(2)}, u32[]{:S(2)}) %all-to-all-start) | async-done | bytes 2097184 | tf_op jit(solution)/shard_map/all_to_all | solution.py:186
  691.0 1.6 copy.113
  692.6 5.8 copy.123
  698.4 2.2 multiply_reduce_fusion
  700.7 12.6 %convolution_convert_fusion = bf16[256,2048]{1,0:T(8,128)(2,1)} fusion(bf16[4096,2048]{1,0:T(8,128)(2,1)} %constant_dynamic-update-slice_fusion, f32[256,4096]{1,0:T(8,128)} %bitcast.124, f32[4096]{0:T(1024)S(1)} %copy-done.23, f32[256]{0:T(256)S(1)} %bitcast.141), kind=kOutput, calls=%fused_computation.45 | convolution fusion | flops 4298637312 | bytes 22037504 | tf_op jit(solution)/shard_map/dot_general | solution.py:189
  (133 shorter events, 36.7 us)
Async XLA Ops:
  6.5 74.1 %copy-start = (bf16[2048,64]{0,1:T(8,128)(2,1)S(1)}, bf16[2048,64]{0,1:T(8,128)(2,1)}, u32[]{:S(2)}) copy-start(bf16[2048,64]{0,1:T(8,128)(2,1)} %param.23) | copy-start | bytes 786436
  6.5 5.7 copy-start.24
  6.5 5.8 copy-start.25
  6.5 5.9 copy-start.15
  6.5 37.4 %copy-start.16 = (bf16[256,128]{1,0:T(8,128)(2,1)S(1)}, bf16[256,128]{1,0:T(8,128)(2,1)}, u32[]{:S(2)}) copy-start(bf16[256,128]{1,0:T(8,128)(2,1)} %param.22) | copy-start | bytes 196612
  6.5 74.1 %all-gather.7.cloned.1.call-start = ((), (), s32[]{:S(2)}) async-start(), calls=%async_computation.1 | async-start | bytes 5242880 | tf_op jit(solution)/shard_map/all_gather | solution.py:111
  10.7 109.9 %all-gather.9.cloned.1.call-start = ((), (), s32[]{:S(2)}) async-start(), calls=%async_computation.2 | async-start | bytes 4718592 | tf_op jit(solution)/shard_map/all_gather | solution.py:92
  11.5 533.1 %all-gather.11.cloned.1.call-start = ((), (), s32[]{:S(2)}) async-start(), calls=%async_computation.3 | async-start | bytes 4718592 | tf_op jit(solution)/shard_map/all_gather | solution.py:91
  12.2 587.0 %all-gather.13.cloned.1.call-start = ((), (), s32[]{:S(2)}) async-start(), calls=%async_computation.4 | async-start | bytes 9437184 | tf_op jit(solution)/shard_map/all_gather | solution.py:31
  88.2 3.7 copy-start.3
  91.8 1.5 copy-start.11
  93.1 1.7 copy-start.13
  129.2 6.4 collective-permute-start
  141.5 8.1 %copy-start.12 = (bf16[1024,128]{1,0:T(8,128)(2,1)S(1)}, bf16[1024,128]{1,0:T(8,128)(2,1)}, u32[]{:S(2)}) copy-start(bf16[1024,128]{1,0:T(8,128)(2,1)} %copy-done.11) | copy-start | bytes 786436
  141.5 8.1 %copy-start.14 = (bf16[1024,128]{1,0:T(8,128)(2,1)S(1)}, bf16[1024,128]{1,0:T(8,128)(2,1)}, u32[]{:S(2)}) copy-start(bf16[1024,128]{1,0:T(8,128)(2,1)} %copy-done.13) | copy-start | bytes 786436
  141.5 8.2 %copy-start.19 = (f32[128]{0:T(128)S(1)}, f32[128]{0:T(128)}, u32[]{:S(2)}) copy-start(f32[128]{0:T(128)} %get-tuple-element.75) | copy-start | bytes 1540
  141.5 8.2 %copy-start.20 = (f32[128]{0:T(128)S(1)}, f32[128]{0:T(128)}, u32[]{:S(2)}) copy-start(f32[128]{0:T(128)} %get-tuple-element.76) | copy-start | bytes 1540
  141.5 8.2 %copy-start.21 = (f32[128]{0:T(128)S(1)}, f32[128]{0:T(128)}, u32[]{:S(2)}) copy-start(f32[128]{0:T(128)} %get-tuple-element.77) | copy-start | bytes 1540
  141.5 8.2 %copy-start.22 = (f32[128]{0:T(128)S(1)}, f32[128]{0:T(128)}, u32[]{:S(2)}) copy-start(f32[128]{0:T(128)} %get-tuple-element.78) | copy-start | bytes 1540
  173.8 11.7 %copy-start.2 = (f32[2,8,16,64,128]{4,3,2,1,0:T(8,128)}, f32[2,8,16,64,128]{4,3,2,1,0:T(8,128)S(1)}, u32[]{:S(2)}) copy-start(f32[2,8,16,64,128]{4,3,2,1,0:T(8,128)S(1)} %fusion.3) | copy-start | bytes 25165828
  173.8 243.5 %copy-start.26 = (f32[64]{0:T(128)S(1)}, f32[64]{0:T(128)}, u32[]{:S(2)}) copy-start(f32[64]{0:T(128)} %param.29) | copy-start | bytes 772
  173.8 243.5 %copy-start.17 = (f32[4,128]{1,0:T(4,128)S(1)}, f32[4,128]{1,0:T(4,128)}, u32[]{:S(2)}) copy-start(f32[4,128]{1,0:T(4,128)} %get-tuple-element.86) | copy-start | bytes 6148
  185.6 78.0 %collective-permute-start.1 = (bf16[4096,256]{1,0:T(8,128)(2,1)}, bf16[4096,256]{1,0:T(8,128)(2,1)S(1)}, u32[]{:S(2)}, u32[]{:S(2)}) collective-permute-start(bf16[4096,256]{1,0:T(8,128)(2,1)} %param.31), channel_id=1, source_target_pairs={{0,4},{4,8},{8,12},{12,16},{16,20},{20,24},{24,28},{28,0},{1,5},{5... | collective-permute-start | bytes 6291464 | tf_op jit(solution)/shard_map/ppermute | solution.py:18
  263.5 1.4 copy-start.5
  264.9 56.0 %collective-permute-start.2 = (bf16[4096,256]{1,0:T(8,128)(2,1)S(1)}, bf16[4096,256]{1,0:T(8,128)(2,1)S(1)}, u32[]{:S(2)}, u32[]{:S(2)}) collective-permute-start(bf16[4096,256]{1,0:T(8,128)(2,1)S(1)} %collective-permute-done.1), channel_id=1, source_target_pairs={{0,4},{4,8},{8,12},{12,16},{16,20},{20,24},{24,28},{28,0},{1,5},{5... | collective-permute-start | bytes 6291464 | tf_op jit(solution)/shard_map/ppermute | solution.py:18
  320.9 1.3 copy-start.7
  322.2 92.2 %collective-permute-start.3 = (bf16[4096,256]{1,0:T(8,128)(2,1)S(1)}, bf16[4096,256]{1,0:T(8,128)(2,1)}, u32[]{:S(2)}, u32[]{:S(2)}) collective-permute-start(bf16[4096,256]{1,0:T(8,128)(2,1)S(1)} %collective-permute-done.2), channel_id=1, source_target_pairs={{0,4},{4,8},{8,12},{12,16},{16,20},{20,24},{24,28},{28,0},{1,5},{5... | collective-permute-start | bytes 6291464 | tf_op jit(solution)/shard_map/ppermute | solution.py:18
  414.5 65.2 %collective-permute-start.4 = (bf16[4096,256]{1,0:T(8,128)(2,1)}, bf16[4096,256]{1,0:T(8,128)(2,1)}, u32[]{:S(2)}, u32[]{:S(2)}) collective-permute-start(bf16[4096,256]{1,0:T(8,128)(2,1)} %collective-permute-done.3), channel_id=1, source_target_pairs={{0,4},{4,8},{8,12},{12,16},{16,20},{20,24},{24,28},{28,0},{1,5},{5... | collective-permute-start | bytes 6291464 | tf_op jit(solution)/shard_map/ppermute | solution.py:18
  479.7 60.5 %collective-permute-start.5 = (bf16[4096,256]{1,0:T(8,128)(2,1)}, bf16[4096,256]{1,0:T(8,128)(2,1)}, u32[]{:S(2)}, u32[]{:S(2)}) collective-permute-start(bf16[4096,256]{1,0:T(8,128)(2,1)} %collective-permute-done.4), channel_id=1, source_target_pairs={{0,4},{4,8},{8,12},{12,16},{16,20},{20,24},{24,28},{28,0},{1,5},{5... | collective-permute-start | bytes 6291464 | tf_op jit(solution)/shard_map/ppermute | solution.py:18
  484.9 6.0 copy-start.4
  490.9 2.3 copy-start.6
  490.9 3.8 copy-start.8
  494.7 4.8 copy-start.18
  540.2 58.9 %collective-permute-start.6 = (bf16[4096,256]{1,0:T(8,128)(2,1)}, bf16[4096,256]{1,0:T(8,128)(2,1)}, u32[]{:S(2)}, u32[]{:S(2)}) collective-permute-start(bf16[4096,256]{1,0:T(8,128)(2,1)} %collective-permute-done.5), channel_id=1, source_target_pairs={{0,4},{4,8},{8,12},{12,16},{16,20},{20,24},{24,28},{28,0},{1,5},{5... | collective-permute-start | bytes 6291464 | tf_op jit(solution)/shard_map/ppermute | solution.py:18
  563.2 18.2 %slice-start = ((s8[8388608]{0:T(1024)(128)(4,1)}), s8[4194304]{0:T(1024)(128)(4,1)S(1)}, s32[]{:S(2)}) async-start(s8[8388608]{0:T(1024)(128)(4,1)} %bitcast.110), calls=%async_computation.5 | async-start | bytes 8388608
  564.1 17.3 %slice-start.1 = ((s8[8388608]{0:T(1024)(128)(4,1)}), s8[4194304]{0:T(1024)(128)(4,1)S(1)}, s32[]{:S(2)}) async-start(s8[8388608]{0:T(1024)(128)(4,1)} %bitcast.110), calls=%async_computation.6 | async-start | bytes 8388608
  599.2 75.5 %collective-permute-start.7 = (bf16[4096,256]{1,0:T(8,128)(2,1)}, bf16[4096,256]{1,0:T(8,128)(2,1)}, u32[]{:S(2)}, u32[]{:S(2)}) collective-permute-start(bf16[4096,256]{1,0:T(8,128)(2,1)} %collective-permute-done.6), channel_id=1, source_target_pairs={{0,4},{4,8},{8,12},{12,16},{16,20},{20,24},{24,28},{28,0},{1,5},{5... | collective-permute-start | bytes 6291464 | tf_op jit(solution)/shard_map/ppermute | solution.py:18
  609.8 9.0 %copy-start.10 = (f32[2,8,64,16]{2,3,1,0:T(8,128)S(1)}, f32[2,8,64,16]{2,3,1,0:T(8,128)}, u32[]{:S(2)}) copy-start(f32[2,8,64,16]{2,3,1,0:T(8,128)} %get-tuple-element.64) | copy-start | bytes 196612
  646.7 8.0 %copy-start.9 = (bf16[1024,1024]{1,0:T(8,128)(2,1)S(1)}, bf16[1024,1024]{1,0:T(8,128)(2,1)}, u32[]{:S(2)}) copy-start(bf16[1024,1024]{1,0:T(8,128)(2,1)} %convolution_convert_fusion.1) | copy-start | bytes 6291460
  661.7 29.2 %all-to-all-start = ((bf16[2,512,1024]{2,0,1:T(2,128)(2,1)}), bf16[2,512,1024]{2,0,1:T(2,128)(2,1)S(1)}, u32[]{:S(2)}, u32[]{:S(2)}) async-start(bf16[2,512,1024]{2,0,1:T(2,128)(2,1)} %copy.112), calls=%async_computation | async-start | bytes 4194304 | tf_op jit(solution)/shard_map/all_to_all | solution.py:186
  692.6 8.1 %copy-start.23 = (f32[4096]{0:T(1024)S(1)}, f32[4096]{0:T(1024)}, u32[]{:S(2)}) copy-start(f32[4096]{0:T(1024)} %param.30) | copy-start | bytes 49156
  700.7 12.6 %copy-start.1 = (bf16[2048,64]{0,1:T(8,128)(2,1)S(1)}, bf16[2048,64]{0,1:T(8,128)(2,1)}, u32[]{:S(2)}) copy-start(bf16[2048,64]{0,1:T(8,128)(2,1)} %param.23) | copy-start | bytes 786436
Sparse Core Ops, SparseCore 0:
  10.8 35.3 all-gather.6
  48.4 72.1 all-gather.8
  122.7 76.7 all-gather.10
  201.5 257.7 all-gather.12
